TPU v7x, 32 devices: a whole 2x2x4 slice. The times are simulated.
32 devices in a mesh: fs: 8 (over z, core), tp: 4 (over y, x).
Axes of the slice: x: 2, y: 2, z: 4, core: 2. Of those that a mesh axis runs over, the one named last changes fastest.
Arguments:
- tokens: bfloat16 [4096, 2048], P('fs'), may hold values from -6 to 6
- cotangent: bfloat16 [4096, 2048], P('fs'), may hold values from -6 to 6
- gate_weight: bfloat16 [2048, 2816], P('fs', 'tp'), may hold values from -0.125 to 0.125
- up_weight: bfloat16 [2048, 2816], P('fs', 'tp'), may hold values from -0.125 to 0.125
- down_weight: bfloat16 [2048, 2816], P('fs', 'tp'), may hold values from -0.109375 to 0.109375
Outputs:
- input_grad: bfloat16 [4096, 2048], P('fs', 'tp')
- gate_grad: float32 [2048, 2816], P('fs', 'tp')
- up_grad: float32 [2048, 2816], P('fs', 'tp')
- down_grad: float32 [2048, 2816], P('fs', 'tp')
All inputs are finite; a program needn't handle non-finite values.
Results may differ from a plain program's by a relative error of at most 0.014.
Values may be sent and summed in bfloat16 or wider, within the bound.
A program may use at most 64 MiB of HBM per device.

v0:
```python
import jax
import jax.numpy as jnp
from jax import lax
from jax.sharding import PartitionSpec as P


def row_product(left, right):
    return lax.dot_general(
        left, right, (((1,), (1,)), ((), ())), preferred_element_type=jnp.float32
    )


def token_product(left, right):
    return lax.dot_general(
        left, right, (((0,), (0,)), ((), ())), preferred_element_type=jnp.float32
    )


def owner_sum(received, groups):
    return received.reshape(groups, received.shape[0] // groups, received.shape[1]).sum(axis=0)


def shards(tokens, cotangent, gate_weight, up_weight, down_weight):
    groups = lax.axis_size("fs")
    whole_gate, whole_up, whole_down = (
        lax.all_gather(gate_weight, "fs", axis=0, tiled=True),
        lax.all_gather(up_weight, "fs", axis=0, tiled=True),
        lax.all_gather(down_weight, "fs", axis=0, tiled=True),
    )
    gate = jnp.dot(tokens, whole_gate, preferred_element_type=jnp.float32)
    up = jnp.dot(tokens, whole_up, preferred_element_type=jnp.float32)
    hidden_grad = jnp.dot(cotangent, whole_down, preferred_element_type=jnp.float32)
    sig = jax.nn.sigmoid(gate)
    act = gate * sig
    hidden = (act * up).astype(jnp.bfloat16)
    gate_cot = (hidden_grad * up * sig * (1.0 + gate * (1.0 - sig))).astype(jnp.bfloat16)
    up_cot = (hidden_grad * act).astype(jnp.bfloat16)
    partial_value = row_product(gate_cot, whole_gate) + row_product(up_cot, whole_up)
    input_grad = lax.psum_scatter(
        partial_value.astype(jnp.bfloat16), "tp", scatter_dimension=1, tiled=True
    )
    gate_term = token_product(tokens, gate_cot)
    gate_grad = owner_sum(
        lax.all_to_all(
            gate_term.astype(jnp.bfloat16), "fs", split_axis=0, concat_axis=0, tiled=True
        ).astype(gate_term.dtype),
        groups,
    )
    up_term = token_product(tokens, up_cot)
    up_grad = owner_sum(
        lax.all_to_all(
            up_term.astype(jnp.bfloat16), "fs", split_axis=0, concat_axis=0, tiled=True
        ).astype(up_term.dtype),
        groups,
    )
    down_term = token_product(cotangent, hidden)
    down_grad = owner_sum(
        lax.all_to_all(
            down_term.astype(jnp.bfloat16), "fs", split_axis=0, concat_axis=0, tiled=True
        ).astype(down_term.dtype),
        groups,
    )
    return (input_grad, gate_grad, up_grad, down_grad)


def solution(mesh):
    in_specs = (P("fs", None), P("fs", None), P("fs", "tp"), P("fs", "tp"), P("fs", "tp"))
    out_specs = (P("fs", "tp"), P("fs", "tp"), P("fs", "tp"), P("fs", "tp"))
    return jax.shard_map(shards, mesh=mesh, in_specs=in_specs, out_specs=out_specs, check_vma=False)
```

profile of v0, /device:TPU:10, one launch (start us, length us, event | category | flops | bytes accessed | tf_op | source)
XLA Modules:
  0.0 328.2 jit_solution(4843245233064751143)
XLA Ops:
  7.2 0.0 copy-start
  7.2 0.0 all-gather.6.cloned.1.call-start
  7.2 0.7 all-gather.6.cloned.1.call-update
  7.9 0.0 all-gather.8.cloned.1.call-start
  8.0 0.7 all-gather.8.cloned.1.call-update
  8.7 0.0 all-gather.4.cloned.1.call-start
  8.7 0.7 all-gather.4.cloned.1.call-update
  9.4 36.4 %all-gather.6.cloned.1.call-done = bf16[2048,704]{0,1:T(8,128)(2,1)} async-done(((bf16[256,704]{0,1:T(8,128)(2,1)}), bf16[2048,704]{0,1:T(8,128)(2,1)}) %all-gather.6.cloned.1.call-update) | async-done | bytes 2883600 | tf_op jit(solution)/shard_map/all_gather | solution.py:27
  45.8 0.0 copy-done
  45.8 3.5 %fusion.3 = f32[512,704]{0,1:T(8,128)S(1)} fusion(bf16[512,2048]{1,0:T(8,128)(2,1)S(1)} %copy-done, bf16[2048,704]{0,1:T(8,128)(2,1)} %all-gather.6.cloned.1.call-done), kind=kOutput, calls=%fused_computation.16 | convolution fusion | flops 1476395008 | bytes 6422528 | tf_op jit(solution)/shard_map/dot_general | solution.py:31
  49.3 0.0 copy-start.3
  49.3 33.3 %all-gather.8.cloned.1.call-done = bf16[2048,704]{0,1:T(8,128)(2,1)} async-done(((bf16[256,704]{0,1:T(8,128)(2,1)}), bf16[2048,704]{0,1:T(8,128)(2,1)}) %all-gather.8.cloned.1.call-update) | async-done | bytes 2883600 | tf_op jit(solution)/shard_map/all_gather | solution.py:26
  82.7 0.0 copy-start.2
  82.7 3.7 %fusion.4 = f32[512,704]{0,1:T(8,128)S(1)} fusion(bf16[512,2048]{1,0:T(8,128)(2,1)S(1)} %copy-done, bf16[2048,704]{0,1:T(8,128)(2,1)} %all-gather.8.cloned.1.call-done), kind=kOutput, calls=%fused_computation.17 | convolution fusion | flops 1476395008 | bytes 6422528 | tf_op jit(solution)/shard_map/dot_general | solution.py:30
  86.3 0.0 copy-done.3
  86.3 0.0 copy-done.2
  86.3 0.0 copy-start.4
  86.3 1.7 convolution_convert_fusion
  88.1 0.0 copy-done.4
  88.1 1.8 copy.18
  89.9 6.8 %all-to-all-start.2 = ((bf16[8,256,704]{1,2,0:T(8,128)(2,1)}), bf16[8,256,704]{1,2,0:T(8,128)(2,1)}, u32[]{:S(2)}, u32[]{:S(2)}) async-start(bf16[8,256,704]{1,2,0:T(8,128)(2,1)} %bitcast.31), calls=%async_computation.3 | async-start | bytes 5767168 | tf_op jit(solution)/shard_map/all_to_all | solution.py:58
  96.7 47.7 %all-gather.4.cloned.1.call-done = bf16[2048,704]{0,1:T(8,128)(2,1)} async-done(((bf16[256,704]{0,1:T(8,128)(2,1)}), bf16[2048,704]{0,1:T(8,128)(2,1)}) %all-gather.4.cloned.1.call-update) | async-done | bytes 2883600 | tf_op jit(solution)/shard_map/all_gather | solution.py:28
  144.4 5.4 %multiply_convert_fusion.1 = (bf16[512,704]{0,1:T(8,128)(2,1)S(1)}, bf16[512,704]{0,1:T(8,128)(2,1)S(1)}) fusion(f32[512,704]{0,1:T(8,128)} %copy-done.4, f32[512,704]{0,1:T(8,128)} %copy-done.3, bf16[512,2048]{1,0:T(8,128)(2,1)} %param.6, bf16[2048,704]{0,1:T(8,128)(2,1)} %all-gather.4.cloned.1.call-done), kind=kOutput, calls=%fused_computation.11 | convolution fusion | flops 1481080832 | bytes 9306112 | tf_op jit(solution)/shard_map/dot_general | solution.py:32
  149.8 1.7 convolution_convert_fusion.1
  151.5 1.7 copy.19
  153.2 24.6 %all-to-all-done.2 = bf16[8,256,704]{1,2,0:T(8,128)(2,1)} async-done(((bf16[8,256,704]{1,2,0:T(8,128)(2,1)}), bf16[8,256,704]{1,2,0:T(8,128)(2,1)}, u32[]{:S(2)}, u32[]{:S(2)}) %all-to-all-start.2) | async-done | bytes 2883616 | tf_op jit(solution)/shard_map/all_to_all | solution.py:58
  177.8 8.0 %all-to-all-start.1 = ((bf16[8,256,704]{1,2,0:T(8,128)(2,1)}), bf16[8,256,704]{1,2,0:T(8,128)(2,1)}, u32[]{:S(2)}, u32[]{:S(2)}) async-start(bf16[8,256,704]{1,2,0:T(8,128)(2,1)} %bitcast.32), calls=%async_computation.2 | async-start | bytes 5767168 | tf_op jit(solution)/shard_map/all_to_all | solution.py:51
  185.8 1.7 convolution_convert_fusion.2
  187.5 1.8 copy.20
  189.3 58.9 %all-to-all-done.1 = bf16[8,256,704]{1,2,0:T(8,128)(2,1)} async-done(((bf16[8,256,704]{1,2,0:T(8,128)(2,1)}), bf16[8,256,704]{1,2,0:T(8,128)(2,1)}, u32[]{:S(2)}, u32[]{:S(2)}) %all-to-all-start.1) | async-done | bytes 2883616 | tf_op jit(solution)/shard_map/all_to_all | solution.py:51
  248.2 7.9 %all-to-all-start = ((bf16[8,256,704]{1,2,0:T(8,128)(2,1)}), bf16[8,256,704]{1,2,0:T(8,128)(2,1)}, u32[]{:S(2)}, u32[]{:S(2)}) async-start(bf16[8,256,704]{1,2,0:T(8,128)(2,1)} %bitcast.30), calls=%async_computation.1 | async-start | bytes 5767168 | tf_op jit(solution)/shard_map/all_to_all | solution.py:44
  256.1 0.0 reduce-scatter.2.cloned.1.call-start
  256.1 0.0 copy-start.1
  256.1 3.8 %fusion.5 = f32[512,2048]{1,0:T(8,128)S(1)} fusion(bf16[512,704]{0,1:T(8,128)(2,1)S(1)} %get-tuple-element.5, bf16[2048,704]{0,1:T(8,128)(2,1)} %all-gather.8.cloned.1.call-done), kind=kOutput, calls=%fused_computation.18 | convolution fusion | flops 1476395008 | bytes 7798784 | tf_op jit(solution)/shard_map/dot_general | solution.py:8
  260.0 0.0 copy-done.1
  260.0 3.3 %add_convert_fusion = bf16[512,2048]{1,0:T(8,128)(2,1)} fusion(f32[512,2048]{1,0:T(8,128)S(1)} %fusion.5, bf16[512,704]{0,1:T(8,128)(2,1)S(1)} %get-tuple-element.4, bf16[2048,704]{0,1:T(8,128)(2,1)S(1)} %copy-done.1), kind=kOutput, calls=%fused_computation.3 | convolution fusion | flops 1478492160 | bytes 9895936 | tf_op jit(solution)/shard_map/dot_general | solution.py:8
  263.3 0.0 reduce-scatter.2.cloned.1.call-update
  263.3 3.1 convert_reduce_fusion
  266.5 3.1 convert_reduce_fusion.1
  269.6 49.0 %all-to-all-done = bf16[8,256,704]{1,2,0:T(8,128)(2,1)} async-done(((bf16[8,256,704]{1,2,0:T(8,128)(2,1)}), bf16[8,256,704]{1,2,0:T(8,128)(2,1)}, u32[]{:S(2)}, u32[]{:S(2)}) %all-to-all-start) | async-done | bytes 2883616 | tf_op jit(solution)/shard_map/all_to_all | solution.py:44
  318.6 3.1 convert_reduce_fusion.2
  321.7 0.0 reduce-scatter.2.cloned.1.call-done
Async XLA Ops:
  7.2 38.6 %copy-start = (bf16[512,2048]{1,0:T(8,128)(2,1)S(1)}, bf16[512,2048]{1,0:T(8,128)(2,1)}, u32[]{:S(2)}) copy-start(bf16[512,2048]{1,0:T(8,128)(2,1)} %param.5) | copy-start | bytes 6291460
  7.2 38.6 %all-gather.6.cloned.1.call-start = ((), (), s32[]{:S(2)}) async-start(), calls=%async_computation.5 | async-start | bytes 3244032 | tf_op jit(solution)/shard_map/all_gather | solution.py:27
  7.9 74.7 %all-gather.8.cloned.1.call-start = ((), (), s32[]{:S(2)}) async-start(), calls=%async_computation.6 | async-start | bytes 3244032 | tf_op jit(solution)/shard_map/all_gather | solution.py:26
  8.7 135.8 %all-gather.4.cloned.1.call-start = ((), (), s32[]{:S(2)}) async-start(), calls=%async_computation.4 | async-start | bytes 3244032 | tf_op jit(solution)/shard_map/all_gather | solution.py:28
  49.3 37.0 %copy-start.3 = (f32[512,704]{0,1:T(8,128)}, f32[512,704]{0,1:T(8,128)S(1)}, u32[]{:S(2)}) copy-start(f32[512,704]{0,1:T(8,128)S(1)} %fusion.3) | copy-start | bytes 4325380
  82.7 3.7 %copy-start.2 = (bf16[512,2048]{1,0:T(8,128)(2,1)S(1)}, bf16[512,2048]{1,0:T(8,128)(2,1)}, u32[]{:S(2)}) copy-start(bf16[512,2048]{1,0:T(8,128)(2,1)} %param.6) | copy-start | bytes 6291460
  86.3 1.7 copy-start.4
  89.9 87.9 %all-to-all-start.2 = ((bf16[8,256,704]{1,2,0:T(8,128)(2,1)}), bf16[8,256,704]{1,2,0:T(8,128)(2,1)}, u32[]{:S(2)}, u32[]{:S(2)}) async-start(bf16[8,256,704]{1,2,0:T(8,128)(2,1)} %bitcast.31), calls=%async_computation.3 | async-start | bytes 5767168 | tf_op jit(solution)/shard_map/all_to_all | solution.py:58
  177.8 70.4 %all-to-all-start.1 = ((bf16[8,256,704]{1,2,0:T(8,128)(2,1)}), bf16[8,256,704]{1,2,0:T(8,128)(2,1)}, u32[]{:S(2)}, u32[]{:S(2)}) async-start(bf16[8,256,704]{1,2,0:T(8,128)(2,1)} %bitcast.32), calls=%async_computation.2 | async-start | bytes 5767168 | tf_op jit(solution)/shard_map/all_to_all | solution.py:51
  248.2 70.3 %all-to-all-start = ((bf16[8,256,704]{1,2,0:T(8,128)(2,1)}), bf16[8,256,704]{1,2,0:T(8,128)(2,1)}, u32[]{:S(2)}, u32[]{:S(2)}) async-start(bf16[8,256,704]{1,2,0:T(8,128)(2,1)} %bitcast.30), calls=%async_computation.1 | async-start | bytes 5767168 | tf_op jit(solution)/shard_map/all_to_all | solution.py:44
  256.1 65.6 %reduce-scatter.2.cloned.1.call-start = ((), (), s32[]{:S(2)}) async-start(), calls=%async_computation.7 | async-start | bytes 2621440 | tf_op jit(solution)/shard_map/reduce_scatter | solution.py:39
  256.1 3.8 %copy-start.1 = (bf16[2048,704]{0,1:T(8,128)(2,1)S(1)}, bf16[2048,704]{0,1:T(8,128)(2,1)}, u32[]{:S(2)}) copy-start(bf16[2048,704]{0,1:T(8,128)(2,1)} %all-gather.6.cloned.1.call-done) | copy-start | bytes 8650756
Sparse Core Ops, SparseCore 0:
  9.6 36.1 all-gather.5
  47.4 35.2 all-gather.7
  84.2 60.1 all-gather.3
  263.5 36.0 reduce-scatter.1
where the time goes:
time: 333 us; the launch traced here: 328 us
  waiting for transfers between devices  252 us (76%)
  matrix products  24.7 us (7%)
  starting transfers between devices  22.8 us (7%)
  between operations  13.9 us (4%)
  other arithmetic  9.38 us (3%)
  local copies, waits for them, and re-layouts  5.39 us (2%)
    all_to_all x1, waiting for transfers between devices, shards(): lax.all_to_all(up_term.astype(jnp.bfloat16), 'fs', split_axis=0, concat_a...  58.9 us
    all_to_all x1, waiting for transfers between devices, shards(): lax.all_to_all(gate_term.astype(jnp.bfloat16), 'fs', split_axis=0, concat...  49 us
    all_gather x1, waiting for transfers between devices, shards(): lax.all_gather(down_weight, 'fs', axis=0, tiled=True)  47.7 us
    all_gather x1, waiting for transfers between devices, shards(): lax.all_gather(up_weight, 'fs', axis=0, tiled=True)  36.4 us
    all_gather x1, waiting for transfers between devices, shards(): lax.all_gather(gate_weight, 'fs', axis=0, tiled=True)  33.3 us
    all_to_all x1, waiting for transfers between devices, shards(): lax.all_to_all(down_term.astype(jnp.bfloat16), 'fs', split_axis=0, concat...  24.6 us
    reduce_sum x3, other arithmetic, owner_sum(): received.reshape(groups, received.shape[0] // groups, received.shape[1])  9.38 us
    all_to_all x1, starting transfers between devices, shards(): lax.all_to_all(up_term.astype(jnp.bfloat16), 'fs', split_axis=0, concat_a...  7.96 us
  transfers between devices with their start and end apart: 7, of which 6 were waited for; matrix products, arithmetic and copies ran while one was open for 12% of the time, Pallas kernels for 0%

commit v1 on v0

--- a/solution.py
+++ b/solution.py
@@ -1,6 +1,10 @@
+import functools
+
 import jax
 import jax.numpy as jnp
 from jax import lax
+from jax.experimental import pallas as pl
+from jax.experimental.pallas import tpu as pltpu
 from jax.sharding import PartitionSpec as P
 
 
@@ -20,7 +24,7 @@
     return received.reshape(groups, received.shape[0] // groups, received.shape[1]).sum(axis=0)
 
 
-def shards(tokens, cotangent, gate_weight, up_weight, down_weight):
+def plain_shards(tokens, cotangent, gate_weight, up_weight, down_weight):
     groups = lax.axis_size("fs")
     whole_gate, whole_up, whole_down = (
         lax.all_gather(gate_weight, "fs", axis=0, tiled=True),
@@ -63,6 +67,389 @@
     return (input_grad, gate_grad, up_grad, down_grad)
 
 
+MESH = pl.DeviceIdType.MESH
+GATE, UP, DOWN = 0, 1, 2
+RIGHT, LEFT, SIBLING = 0, 1, 2
+
+
+def kernel(
+    n, n_tp, tok, cot, gw, uw, dw, ig_out, out,
+    x, w_all, acc, cots, sib_out, sib_in, line_out, line_in, total, ig_part, ig_in,
+    local_sem, ag_send, ag_recv, sib_send, sib_recv, line_send, line_recv, ig_send, ig_recv,
+):
+    me, tp = lax.axis_index("fs"), lax.axis_index("tp")
+    z, c = me // 2, me % 2
+    nz = n // 2
+    other = 2 * z + 1 - c
+    rows = gw.shape[0]
+    own_columns = ig_out.shape[1]
+    pieces = own_columns // rows
+    has_left, has_right = z > 0, z < nz - 1
+    is_end = jnp.logical_or(z == 0, z == nz - 1)
+
+    loads = [
+        pltpu.make_async_copy(gw, w_all.at[GATE, me], local_sem.at[0]),
+        pltpu.make_async_copy(uw, w_all.at[UP, me], local_sem.at[1]),
+        pltpu.make_async_copy(dw, w_all.at[DOWN, me], local_sem.at[2]),
+        pltpu.make_async_copy(tok, x.at[0], local_sem.at[3]),
+        pltpu.make_async_copy(cot, x.at[1], local_sem.at[4]),
+    ]
+    for load in loads:
+        load.start()
+
+    barrier = pltpu.get_barrier_semaphore()
+    pl.semaphore_signal(barrier, inc=1, device_id={"fs": other}, device_id_type=MESH)
+    for step in range(1, n_tp):
+        pl.semaphore_signal(
+            barrier, inc=1, device_id={"tp": lax.rem(tp + step, n_tp)}, device_id_type=MESH
+        )
+
+    @pl.when(has_right)
+    def _():
+        pl.semaphore_signal(barrier, inc=1, device_id={"fs": me + 2}, device_id_type=MESH)
+
+    @pl.when(has_left)
+    def _():
+        pl.semaphore_signal(barrier, inc=1, device_id={"fs": me - 2}, device_id_type=MESH)
+
+    pl.semaphore_wait(barrier, n_tp + has_left.astype(jnp.int32) + has_right.astype(jnp.int32))
+
+    def gather_copy(w, chip, way):
+        slot = 2 * chip + c
+        device = (me + 2, me - 2, other)[way]
+        return pltpu.make_async_remote_copy(
+            src_ref=w_all.at[w, slot], dst_ref=w_all.at[w, slot],
+            send_sem=ag_send.at[w, way, chip], recv_sem=ag_recv.at[w, slot],
+            device_id={"fs": device}, device_id_type=MESH,
+        )
+
+    def gather_wait(w, slot):
+        pltpu.make_async_remote_copy(
+            src_ref=w_all.at[w, slot], dst_ref=w_all.at[w, slot],
+            send_sem=ag_send.at[w, SIBLING, 0], recv_sem=ag_recv.at[w, slot],
+            device_id={"fs": other}, device_id_type=MESH,
+        ).wait_recv()
+
+    for w in range(3):
+        loads[w].wait()
+        if w == 0:
+
+            @pl.when(has_right)
+            def _():
+                gather_copy(GATE, z, RIGHT).start()
+
+            @pl.when(has_left)
+            def _():
+                gather_copy(GATE, z, LEFT).start()
+
+        gather_copy(w, z, SIBLING).start()
+    acc[...] = jnp.zeros_like(acc)
+    loads[3].wait()
+    loads[4].wait()
+
+    def gather_step(w, s):
+        @pl.when(jnp.logical_and(s > 0, z - s >= 0))
+        def _():
+            gather_wait(w, me - 2 * s)
+
+            @pl.when(has_right)
+            def _():
+                gather_copy(w, z - s, RIGHT).start()
+
+            gather_copy(w, z - s, SIBLING).start()
+
+        @pl.when(jnp.logical_and(s > 0, z + s < nz))
+        def _():
+            gather_wait(w, me + 2 * s)
+
+            @pl.when(has_left)
+            def _():
+                gather_copy(w, z + s, LEFT).start()
+
+            gather_copy(w, z + s, SIBLING).start()
+
+        @pl.when(jnp.logical_and(w < DOWN, jnp.logical_and(has_right, s == z)))
+        def _():
+            gather_copy(w + 1, z, RIGHT).start()
+
+        @pl.when(jnp.logical_and(w < DOWN, jnp.logical_and(has_left, s == nz - 1 - z)))
+        def _():
+            gather_copy(w + 1, z, LEFT).start()
+
+        def block(j, carry):
+            way, core = j % 2, j // 2
+            chip = z + s * (2 * way - 1)
+            here = jnp.logical_and(jnp.logical_and(chip >= 0, chip < nz), way * 1 <= s)
+            slot = 2 * chip + core * (1 - c) + (1 - core) * c
+
+            @pl.when(here)
+            def _():
+                @pl.when(core == 1)
+                def _():
+                    gather_wait(w, slot)
+
+                columns = pl.ds(pl.multiple_of(slot * rows, rows), rows)
+                acc[w] += jnp.dot(
+                    x[w // 2, :, columns], w_all[w, slot], preferred_element_type=jnp.float32
+                )
+
+            return carry
+
+        lax.fori_loop(0, 4, block, 0)
+
+    def gather(w):
+        def body(s, carry):
+            gather_step(w, s)
+            return carry
+
+        lax.fori_loop(0, nz, body, 0)
+
+    def by_rows(body):
+        height = 32
+
+        def step(i, carry):
+            body(pl.ds(pl.multiple_of(i * height, height), height))
+            return carry
+
+        lax.fori_loop(0, x.shape[1] // height, step, 0)
+
+    def term(g, slot):
+        columns = pl.ds(pl.multiple_of(slot * rows, rows), rows)
+        return token_product(x[g // 2, :, columns], cots[g])
+
+    def sibling_copy(g, chip):
+        return pltpu.make_async_remote_copy(
+            src_ref=sib_out.at[g, chip], dst_ref=sib_in.at[g, chip],
+            send_sem=sib_send.at[g, chip], recv_sem=sib_recv.at[g, chip],
+            device_id={"fs": other}, device_id_type=MESH,
+        )
+
+    def line_copy(g, way, chip):
+        return pltpu.make_async_remote_copy(
+            src_ref=line_out.at[g, chip], dst_ref=line_in.at[g, way, chip],
+            send_sem=line_send.at[g, chip], recv_sem=line_recv.at[g, way, chip],
+            device_id={"fs": me + 2 - 4 * way}, device_id_type=MESH,
+        )
+
+    def pair_sum(g, chip):
+        sib_out[g, chip] = term(g, 2 * chip + 1 - c).astype(jnp.bfloat16)
+        sibling_copy(g, chip).start()
+        own = term(g, 2 * chip + c)
+        sibling_copy(g, chip).wait_recv()
+        return own + sib_in[g, chip].astype(jnp.float32)
+
+    def reduce_step(g, k):
+        def one(j, carry):
+            way = jnp.where(z * 2 >= nz, 1 - j, j)
+            chip = jnp.where(way == RIGHT, nz - k, k - 1)
+            active = jnp.where(way == RIGHT, chip - z, z - chip) > 0
+            behind = jnp.where(way == RIGHT, z, nz - 1 - z) > 0
+
+            @pl.when(active)
+            def _():
+                total[...] = pair_sum(g, chip)
+
+                @pl.when(behind)
+                def _():
+                    line_copy(g, way, chip).wait_recv()
+                    total[...] += line_in[g, way, chip].astype(jnp.float32)
+
+                line_out[g, chip] = total[...].astype(jnp.bfloat16)
+                line_copy(g, way, chip).start()
+
+            return carry
+
+        lax.fori_loop(0, 2, one, 0)
+
+    def reduce_own(g):
+        out[g] = pair_sum(g, z)
+
+    def reduce_final(g):
+        @pl.when(has_left)
+        def _():
+            line_copy(g, RIGHT, z).wait_recv()
+            out[g] += line_in[g, RIGHT, z].astype(jnp.float32)
+
+        @pl.when(has_right)
+        def _():
+            line_copy(g, LEFT, z).wait_recv()
+            out[g] += line_in[g, LEFT, z].astype(jnp.float32)
+
+    def reduce_down(now):
+        @pl.when(now)
+        def _():
+            def body(k, carry):
+                reduce_step(DOWN, k)
+                return carry
+
+            lax.fori_loop(1, nz, body, 0)
+
+    def input_copy(peer, source):
+        return pltpu.make_async_remote_copy(
+            src_ref=ig_part.at[peer], dst_ref=ig_in.at[source],
+            send_sem=ig_send.at[peer], recv_sem=ig_recv.at[source],
+            device_id={"tp": peer}, device_id_type=MESH,
+        )
+
+    def input_part(step):
+        peer = lax.rem(tp + 1 + step, n_tp)
+
+        def piece(i, carry):
+            slot = peer * pieces + i
+            value = row_product(cots[GATE], w_all[GATE, slot])
+            value = value + row_product(cots[UP], w_all[UP, slot])
+            ig_part[peer, :, pl.ds(pl.multiple_of(i * rows, rows), rows)] = value.astype(jnp.bfloat16)
+            return carry
+
+        lax.fori_loop(0, pieces, piece, 0)
+
+        @pl.when(step < n_tp - 1)
+        def _():
+            input_copy(peer, tp).start()
+
+    def first_two(w, carry):
+        gather(w)
+        return carry
+
+    lax.fori_loop(0, 2, first_two, 0)
+
+    def make_hidden(r):
+        gate = acc[GATE, r, :]
+        sig = jax.nn.sigmoid(gate)
+        act = gate * sig
+        up = acc[UP, r, :]
+        cots[DOWN, r, :] = (act * up).astype(jnp.bfloat16)
+        acc[UP, r, :] = up * sig * (1.0 + gate * (1.0 - sig))
+        acc[GATE, r, :] = act
+
+    by_rows(make_hidden)
+    reduce_down(is_end)
+    gather(DOWN)
+    reduce_down(jnp.logical_not(is_end))
+
+    def make_cots(r):
+        hidden_grad = acc[DOWN, r, :]
+        cots[GATE, r, :] = (hidden_grad * acc[UP, r, :]).astype(jnp.bfloat16)
+        cots[UP, r, :] = (hidden_grad * acc[GATE, r, :]).astype(jnp.bfloat16)
+
+    by_rows(make_cots)
+
+    def last_two(t, carry):
+        @pl.when(t < 2 * (nz - 1))
+        def _():
+            reduce_step(t // max(nz - 1, 1), t % max(nz - 1, 1) + 1)
+
+        @pl.when(t < n_tp)
+        def _():
+            input_part(t)
+
+        return carry
+
+    lax.fori_loop(0, max(2 * (nz - 1), n_tp), last_two, 0)
+
+    def owns(g, carry):
+        reduce_own(g)
+        return carry
+
+    lax.fori_loop(0, 3, owns, 0)
+
+    ig_in[tp] = ig_part[tp]
+    for step in range(1, n_tp):
+        source = lax.rem(tp + step, n_tp)
+        input_copy(source, source).wait_recv()
+    for half in range(2):
+        height = ig_out.shape[0] // 2
+        r = pl.ds(half * height, height)
+        value = ig_in[0, r, :].astype(jnp.float32)
+        for source in range(1, n_tp):
+            value = value + ig_in[source, r, :].astype(jnp.float32)
+        ig_out[r, :] = value.astype(ig_out.dtype)
+
+    def finals(i, carry):
+        reduce_final(lax.rem(i + 2, 3))
+        return carry
+
+    lax.fori_loop(0, 3, finals, 0)
+
+    def drain(i, carry):
+        g, chip = i // nz, i % nz
+        gather_copy(g, chip, SIBLING).wait_send()
+        sibling_copy(g, chip).wait_send()
+
+        @pl.when(jnp.logical_and(has_right, chip <= z))
+        def _():
+            gather_copy(g, chip, RIGHT).wait_send()
+
+        @pl.when(jnp.logical_and(has_left, chip >= z))
+        def _():
+            gather_copy(g, chip, LEFT).wait_send()
+
+        @pl.when(chip != z)
+        def _():
+            way = jnp.where(chip > z, RIGHT, LEFT)
+            line_copy(g, way, chip).wait_send()
+
+        return carry
+
+    lax.fori_loop(0, 3 * nz, drain, 0)
+    for step in range(1, n_tp):
+        input_copy(lax.rem(tp + step, n_tp), tp).wait_send()
+
+
+def fused_shards(tokens, cotangent, gate_weight, up_weight, down_weight):
+    n, n_tp = lax.axis_size("fs"), lax.axis_size("tp")
+    nz = n // 2
+    count, width = tokens.shape
+    rows, hidden = gate_weight.shape
+    share = width // n_tp
+    bf16, f32 = jnp.bfloat16, jnp.float32
+    dma = pltpu.SemaphoreType.DMA
+    input_grad, grads = pl.pallas_call(
+        functools.partial(kernel, n, n_tp),
+        out_shape=(
+            jax.ShapeDtypeStruct((count, share), bf16),
+            jax.ShapeDtypeStruct((3, rows, hidden), f32),
+        ),
+        in_specs=[pl.BlockSpec(memory_space=pl.ANY)] * 5,
+        out_specs=(pl.BlockSpec(memory_space=pltpu.VMEM),) * 2,
+        scratch_shapes=[
+            pltpu.VMEM((2, count, width), bf16),
+            pltpu.VMEM((3, n, rows, hidden), bf16),
+            pltpu.VMEM((3, count, hidden), f32),
+            pltpu.VMEM((3, count, hidden), bf16),
+            pltpu.VMEM((3, nz, rows, hidden), bf16),
+            pltpu.VMEM((3, nz, rows, hidden), bf16),
+            pltpu.VMEM((3, nz, rows, hidden), bf16),
+            pltpu.VMEM((3, 2, nz, rows, hidden), bf16),
+            pltpu.VMEM((rows, hidden), f32),
+            pltpu.VMEM((n_tp, count, share), bf16),
+            pltpu.VMEM((n_tp, count, share), bf16),
+            dma((5,)),
+            dma((3, 3, nz)),
+            dma((3, n)),
+            dma((3, nz)),
+            dma((3, nz)),
+            dma((3, nz)),
+            dma((3, 2, nz)),
+            dma((n_tp,)),
+            dma((n_tp,)),
+        ],
+        compiler_params=pltpu.CompilerParams(
+            collective_id=0, has_side_effects=True, vmem_limit_bytes=67043328
+        ),
+    )(tokens, cotangent, gate_weight, up_weight, down_weight)
+    return input_grad, grads[0], grads[1], grads[2]
+
+
+def shards(tokens, cotangent, gate_weight, up_weight, down_weight):
+    n, n_tp = lax.axis_size("fs"), lax.axis_size("tp")
+    rows = gate_weight.shape[0]
+    share = tokens.shape[1] // n_tp
+    if n % 2 == 0 and rows % 128 == 0 and share % rows == 0 and n <= 8:
+        return fused_shards(tokens, cotangent, gate_weight, up_weight, down_weight)
+    return plain_shards(tokens, cotangent, gate_weight, up_weight, down_weight)
+
+
 def solution(mesh):
     in_specs = (P("fs", None), P("fs", None), P("fs", "tp"), P("fs", "tp"), P("fs", "tp"))
     out_specs = (P("fs", "tp"), P("fs", "tp"), P("fs", "tp"), P("fs", "tp"))

time: 333 us -> 165 us (0.50)
  waiting for transfers between devices: 252 us -> 0 us
  Pallas kernels: 0 us -> 151 us
  matrix products: 24.7 us -> 0 us
  starting transfers between devices: 22.8 us -> 0 us
  between operations: 13.9 us -> 0.65 us
  other arithmetic: 9.38 us -> 0 us
  local copies, waits for them, and re-layouts: 5.39 us -> 11.6 us
    pallas_call x0 -> x1, Pallas kernels: none -> 151 us  [fused_shards(): pl.pallas_call(functools.partial(kernel, n, n_tp), out_shape=(jax.ShapeDt...]
    all_to_all x3 -> x0, waiting for transfers between devices: 133 us -> none  [the longest x1 58.9 us: shards(): lax.all_to_all(up_term.astype(jnp.bfloat16), 'fs', split_axis=0, concat_a...]
    all_gather x3 -> x0, waiting for transfers between devices: 117 us -> none  [the longest x1 47.7 us: shards(): lax.all_gather(down_weight, 'fs', axis=0, tiled=True)]
    dot_general x8 -> x0, matrix products: 24.7 us -> none  [the longest x2 7.16 us: row_product(): lax.dot_general(left, right, (((1,), (1,)), ((), ())), preferred_element_...]
    all_to_all x3 -> x0, starting transfers between devices: 22.7 us -> none  [the longest x1 7.96 us: shards(): lax.all_to_all(up_term.astype(jnp.bfloat16), 'fs', split_axis=0, concat_a...]
    unnamed x10 -> x9, local copies, waits for them, and re-layouts: 0.03 us -> 9.84 us
    reduce_sum x3 -> x0, other arithmetic: 9.38 us -> none  [owner_sum(): received.reshape(groups, received.shape[0] // groups, received.shape[1])]
    all_to_all x3 -> x0, local copies, waits for them, and re-layouts: 5.37 us -> none  [the longest x1 1.83 us: shards(): lax.all_to_all(gate_term.astype(jnp.bfloat16), 'fs', split_axis=0, concat...]
  transfers between devices with their start and end apart: 7 -> 0, of which waited for: 6 -> 0; matrix products, arithmetic and copies ran while one was open for 12% -> 0% of each run, Pallas kernels for 0% -> 0%
where the time goes in v1:
time: 165 us; the launch traced here: 163 us
  Pallas kernels  151 us (92%)
  local copies, waits for them, and re-layouts  11.6 us (7%)
    pallas_call x1, Pallas kernels, fused_shards(): pl.pallas_call(functools.partial(kernel, n, n_tp), out_shape=(jax.ShapeDt...  151 us
    unnamed x9, local copies, waits for them, and re-layouts  9.84 us

profile of v1, /device:TPU:10, one launch (start us, length us, event | category | flops | bytes accessed | tf_op | source)
XLA Modules:
  0.0 162.8 jit_solution(4516524599779983444)
XLA Ops:
  0.6 1.9 %copy.9.gw = bf16[256,704]{1,0:T(8,128)(2,1)} copy(bf16[256,704]{0,1:T(8,128)(2,1)} %param.7) | data formatting | bytes 720896 | tf_op args[2]
  2.5 1.9 %copy.10.uw = bf16[256,704]{1,0:T(8,128)(2,1)} copy(bf16[256,704]{0,1:T(8,128)(2,1)} %param.8) | data formatting | bytes 720896 | tf_op args[3]
  4.4 1.9 %copy.11.dw = bf16[256,704]{1,0:T(8,128)(2,1)} copy(bf16[256,704]{0,1:T(8,128)(2,1)} %param.9) | data formatting | bytes 720896 | tf_op args[4]
  6.3 150.6 %shard_map.84 = (bf16[512,512]{1,0:T(8,128)(2,1)}, f32[3,256,704]{2,1,0:T(8,128)}) custom-call(bf16[512,2048]{1,0:T(8,128)(2,1)} %tok.1, bf16[512,2048]{1,0:T(8,128)(2,1)} %cot.1, bf16[256,704]{1,0:T(8,128)(2,1)} %copy.9.gw, bf16[256,704]{1,0:T(8,128)(2,1)} %copy.10.uw, bf16[256,704]{1,0:T(8,128)(2,1)} %copy.11.dw), custom_call_target="tpu_custom_call" | custom-call | tf_op jit(solution)/shard_map/pallas_call | solution.py:407
  156.9 1.8 %slice_bitcast_fusion = (f32[256,704]{1,0:T(8,128)S(1)}, f32[256,704]{1,0:T(8,128)S(1)}, f32[256,704]{1,0:T(8,128)S(1)}) fusion(f32[3,256,704]{2,1,0:T(8,128)} %get-tuple-element.7), kind=kLoop, calls=%fused_computation | loop fusion | bytes 4325376 | tf_op jit(solution)/shard_map/squeeze | solution.py:441
  158.7 0.0 copy-start
  158.7 1.1 copy.14
  159.8 1.1 copy.13
  160.9 1.1 copy.12
  162.0 0.0 copy-done
  162.0 0.8 copy.16
Async XLA Ops:
  158.7 3.3 %copy-start = (bf16[512,512]{1,0:T(8,128)(2,1)S(1)}, bf16[512,512]{1,0:T(8,128)(2,1)}, u32[]{:S(2)}) copy-start(bf16[512,512]{1,0:T(8,128)(2,1)} %get-tuple-element.19) | copy-start | bytes 1572868

commit v2 on v1

--- a/solution.py
+++ b/solution.py
@@ -73,26 +73,31 @@
 
 
 def kernel(
-    n, n_tp, tok, cot, gw, uw, dw, ig_out, out,
-    x, w_all, acc, cots, sib_out, sib_in, line_out, line_in, total, ig_part, ig_in,
+    n, n_tp, parts, tok, cot, gw, uw, dw, ig_out, gate_out, up_out, down_out,
+    x, w_all, acc, cots, own_sum, sib_out, sib_in, line_out, line_in, total, ig_part, ig_in,
     local_sem, ag_send, ag_recv, sib_send, sib_recv, line_send, line_recv, ig_send, ig_recv,
 ):
     me, tp = lax.axis_index("fs"), lax.axis_index("tp")
     z, c = me // 2, me % 2
     nz = n // 2
     other = 2 * z + 1 - c
-    rows = gw.shape[0]
+    rows = gw.shape[1]
+    height = gw.shape[0] // parts
     own_columns = ig_out.shape[1]
     pieces = own_columns // rows
     has_left, has_right = z > 0, z < nz - 1
     is_end = jnp.logical_or(z == 0, z == nz - 1)
 
-    loads = [
-        pltpu.make_async_copy(gw, w_all.at[GATE, me], local_sem.at[0]),
-        pltpu.make_async_copy(uw, w_all.at[UP, me], local_sem.at[1]),
-        pltpu.make_async_copy(dw, w_all.at[DOWN, me], local_sem.at[2]),
-        pltpu.make_async_copy(tok, x.at[0], local_sem.at[3]),
-        pltpu.make_async_copy(cot, x.at[1], local_sem.at[4]),
+    def weight_load(t):
+        piece = pl.ds((t // 3) * height, height)
+        return pltpu.make_async_copy(
+            (gw, uw, dw)[t % 3].at[piece, :], w_all.at[t, me], local_sem.at[t]
+        )
+
+    loads = [weight_load(t) for t in range(3 * parts)]
+    loads += [
+        pltpu.make_async_copy(tok, x.at[0], local_sem.at[3 * parts]),
+        pltpu.make_async_copy(cot, x.at[1], local_sem.at[3 * parts + 1]),
     ]
     for load in loads:
         load.start()
@@ -130,22 +135,20 @@
             device_id={"fs": other}, device_id_type=MESH,
         ).wait_recv()
 
-    for w in range(3):
-        loads[w].wait()
-        if w == 0:
-
-            @pl.when(has_right)
-            def _():
-                gather_copy(GATE, z, RIGHT).start()
-
-            @pl.when(has_left)
-            def _():
-                gather_copy(GATE, z, LEFT).start()
-
-        gather_copy(w, z, SIBLING).start()
-    acc[...] = jnp.zeros_like(acc)
-    loads[3].wait()
-    loads[4].wait()
+    for t in range(3 * parts):
+        loads[t].wait()
+
+        @pl.when(jnp.logical_and(has_right, jnp.logical_or(z == 0, t == 0)))
+        def _():
+            gather_copy(t, z, RIGHT).start()
+
+        @pl.when(jnp.logical_and(has_left, jnp.logical_or(z == nz - 1, t == 0)))
+        def _():
+            gather_copy(t, z, LEFT).start()
+
+        gather_copy(t, z, SIBLING).start()
+    loads[3 * parts].wait()
+    loads[3 * parts + 1].wait()
 
     def gather_step(w, s):
         @pl.when(jnp.logical_and(s > 0, z - s >= 0))
@@ -168,11 +171,13 @@
 
             gather_copy(w, z + s, SIBLING).start()
 
-        @pl.when(jnp.logical_and(w < DOWN, jnp.logical_and(has_right, s == z)))
+        more = jnp.logical_and(w < 3 * parts - 1, jnp.logical_not(is_end))
+
+        @pl.when(jnp.logical_and(more, s == z))
         def _():
             gather_copy(w + 1, z, RIGHT).start()
 
-        @pl.when(jnp.logical_and(w < DOWN, jnp.logical_and(has_left, s == nz - 1 - z)))
+        @pl.when(jnp.logical_and(more, s == nz - 1 - z))
         def _():
             gather_copy(w + 1, z, LEFT).start()
 
@@ -189,9 +194,8 @@
                     gather_wait(w, slot)
 
                 columns = pl.ds(pl.multiple_of(slot * rows, rows), rows)
-                acc[w] += jnp.dot(
-                    x[w // 2, :, columns], w_all[w, slot], preferred_element_type=jnp.float32
-                )
+                kind = w % 3
+                acc[kind] += row_product(w_all[w, slot], x[kind // 2, :, columns])
 
             return carry
 
@@ -205,17 +209,19 @@
         lax.fori_loop(0, nz, body, 0)
 
     def by_rows(body):
-        height = 32
+        strip = 16
 
         def step(i, carry):
-            body(pl.ds(pl.multiple_of(i * height, height), height))
+            body(pl.ds(pl.multiple_of(i * strip, strip), strip))
             return carry
 
-        lax.fori_loop(0, x.shape[1] // height, step, 0)
+        lax.fori_loop(0, height // strip, step, 0)
 
     def term(g, slot):
         columns = pl.ds(pl.multiple_of(slot * rows, rows), rows)
-        return token_product(x[g // 2, :, columns], cots[g])
+        return jnp.dot(
+            cots[g], x[(g % 3) // 2, :, columns], preferred_element_type=jnp.float32
+        )
 
     def sibling_copy(g, chip):
         return pltpu.make_async_remote_copy(
@@ -231,58 +237,80 @@
             device_id={"fs": me + 2 - 4 * way}, device_id_type=MESH,
         )
 
-    def pair_sum(g, chip):
+    def sibling_term(g, chip):
         sib_out[g, chip] = term(g, 2 * chip + 1 - c).astype(jnp.bfloat16)
         sibling_copy(g, chip).start()
+
+    def pair_sum(g, chip):
         own = term(g, 2 * chip + c)
         sibling_copy(g, chip).wait_recv()
         return own + sib_in[g, chip].astype(jnp.float32)
 
-    def reduce_step(g, k):
+    def each_way(k, body):
         def one(j, carry):
             way = jnp.where(z * 2 >= nz, 1 - j, j)
             chip = jnp.where(way == RIGHT, nz - k, k - 1)
             active = jnp.where(way == RIGHT, chip - z, z - chip) > 0
-            behind = jnp.where(way == RIGHT, z, nz - 1 - z) > 0
 
             @pl.when(active)
             def _():
-                total[...] = pair_sum(g, chip)
-
-                @pl.when(behind)
-                def _():
-                    line_copy(g, way, chip).wait_recv()
-                    total[...] += line_in[g, way, chip].astype(jnp.float32)
-
-                line_out[g, chip] = total[...].astype(jnp.bfloat16)
-                line_copy(g, way, chip).start()
+                body(way, chip)
 
             return carry
 
         lax.fori_loop(0, 2, one, 0)
 
+    def sibling_terms(g):
+        def body(k, carry):
+            each_way(k, lambda way, chip: sibling_term(g, chip))
+            return carry
+
+        lax.fori_loop(1, nz, body, 0)
+        sibling_term(g, z)
+
+    def reduce_step(g, k):
+        def one(way, chip):
+            behind = jnp.where(way == RIGHT, z, nz - 1 - z) > 0
+            total[...] = pair_sum(g, chip)
+
+            @pl.when(behind)
+            def _():
+                line_copy(g, way, chip).wait_recv()
+                total[...] += line_in[g, way, chip].astype(jnp.float32)
+
+            line_out[g, chip] = total[...].astype(jnp.bfloat16)
+            line_copy(g, way, chip).start()
+
+        each_way(k, one)
+
     def reduce_own(g):
-        out[g] = pair_sum(g, z)
+        own_sum[g] = pair_sum(g, z)
 
     def reduce_final(g):
         @pl.when(has_left)
         def _():
             line_copy(g, RIGHT, z).wait_recv()
-            out[g] += line_in[g, RIGHT, z].astype(jnp.float32)
+            own_sum[g] += line_in[g, RIGHT, z].astype(jnp.float32)
 
         @pl.when(has_right)
         def _():
             line_copy(g, LEFT, z).wait_recv()
-            out[g] += line_in[g, LEFT, z].astype(jnp.float32)
-
-    def reduce_down(now):
+            own_sum[g] += line_in[g, LEFT, z].astype(jnp.float32)
+
+        piece = pl.ds((g // 3) * height, height)
+        (gate_out, up_out, down_out)[g % 3][piece, :] = own_sum[g]
+
+    def reduce_all(g, now):
         @pl.when(now)
         def _():
+            sibling_terms(g)
+
             def body(k, carry):
-                reduce_step(DOWN, k)
+                reduce_step(g, k)
                 return carry
 
             lax.fori_loop(1, nz, body, 0)
+            reduce_own(g)
 
     def input_copy(peer, source):
         return pltpu.make_async_remote_copy(
@@ -296,8 +324,9 @@
 
         def piece(i, carry):
             slot = peer * pieces + i
-            value = row_product(cots[GATE], w_all[GATE, slot])
-            value = value + row_product(cots[UP], w_all[UP, slot])
+            value = token_product(cots[GATE], w_all[GATE, slot])
+            for t in [t for t in range(1, 3 * parts) if t % 3 != DOWN]:
+                value = value + token_product(cots[t], w_all[t, slot])
             ig_part[peer, :, pl.ds(pl.multiple_of(i * rows, rows), rows)] = value.astype(jnp.bfloat16)
             return carry
 
@@ -307,69 +336,84 @@
         def _():
             input_copy(peer, tp).start()
 
-    def first_two(w, carry):
-        gather(w)
+    def make_hidden(t):
+        def strip(r):
+            gate = acc[GATE, r, :]
+            sig = jax.nn.sigmoid(gate)
+            act = gate * sig
+            up = acc[UP, r, :]
+            cots[t + 1, r, :] = (act * up).astype(jnp.bfloat16)
+            acc[UP, r, :] = up * sig * (1.0 + gate * (1.0 - sig))
+            acc[GATE, r, :] = act
+
+        by_rows(strip)
+
+    def make_cots(t):
+        def strip(r):
+            hidden_grad = acc[DOWN, r, :]
+            cots[t - 2, r, :] = (hidden_grad * acc[UP, r, :]).astype(jnp.bfloat16)
+            cots[t - 1, r, :] = (hidden_grad * acc[GATE, r, :]).astype(jnp.bfloat16)
+
+        by_rows(strip)
+
+    def gather_and_reduce(t, carry):
+        kind = t % 3
+        g = jnp.where(kind == DOWN, t, t - 3)
+        acc[kind] = jnp.zeros(acc.shape[1:], acc.dtype)
+        reduce_all(g, jnp.logical_and(g >= 0, is_end))
+        gather(t)
+        reduce_all(g, jnp.logical_and(g >= 0, jnp.logical_not(is_end)))
+
+        @pl.when(kind == UP)
+        def _():
+            make_hidden(t)
+
+        @pl.when(kind == DOWN)
+        def _():
+            make_cots(t)
+
         return carry
 
-    lax.fori_loop(0, 2, first_two, 0)
-
-    def make_hidden(r):
-        gate = acc[GATE, r, :]
-        sig = jax.nn.sigmoid(gate)
-        act = gate * sig
-        up = acc[UP, r, :]
-        cots[DOWN, r, :] = (act * up).astype(jnp.bfloat16)
-        acc[UP, r, :] = up * sig * (1.0 + gate * (1.0 - sig))
-        acc[GATE, r, :] = act
-
-    by_rows(make_hidden)
-    reduce_down(is_end)
-    gather(DOWN)
-    reduce_down(jnp.logical_not(is_end))
-
-    def make_cots(r):
-        hidden_grad = acc[DOWN, r, :]
-        cots[GATE, r, :] = (hidden_grad * acc[UP, r, :]).astype(jnp.bfloat16)
-        cots[UP, r, :] = (hidden_grad * acc[GATE, r, :]).astype(jnp.bfloat16)
-
-    by_rows(make_cots)
-
-    def last_two(t, carry):
-        @pl.when(t < 2 * (nz - 1))
-        def _():
-            reduce_step(t // max(nz - 1, 1), t % max(nz - 1, 1) + 1)
-
-        @pl.when(t < n_tp)
-        def _():
-            input_part(t)
+    lax.fori_loop(0, 3 * parts, gather_and_reduce, 0)
+    last = 3 * parts - 3
+    steps = max(nz - 1, 1)
+
+    def last_two(i, carry):
+        g = last + i // steps
+
+        @pl.when(jnp.logical_and(i < 2 * steps, i % steps == 0))
+        def _():
+            sibling_terms(g)
+
+        @pl.when(i < 2 * (nz - 1))
+        def _():
+            reduce_step(g, i % steps + 1)
+
+        @pl.when(i < n_tp)
+        def _():
+            input_part(i)
 
         return carry
 
-    lax.fori_loop(0, max(2 * (nz - 1), n_tp), last_two, 0)
-
-    def owns(g, carry):
-        reduce_own(g)
-        return carry
-
-    lax.fori_loop(0, 3, owns, 0)
+    lax.fori_loop(0, max(2 * steps, n_tp), last_two, 0)
+    reduce_own(last)
+    reduce_own(last + 1)
 
     ig_in[tp] = ig_part[tp]
     for step in range(1, n_tp):
         source = lax.rem(tp + step, n_tp)
         input_copy(source, source).wait_recv()
     for half in range(2):
-        height = ig_out.shape[0] // 2
-        r = pl.ds(half * height, height)
+        strip = ig_out.shape[0] // 2
+        r = pl.ds(half * strip, strip)
         value = ig_in[0, r, :].astype(jnp.float32)
         for source in range(1, n_tp):
             value = value + ig_in[source, r, :].astype(jnp.float32)
         ig_out[r, :] = value.astype(ig_out.dtype)
 
-    def finals(i, carry):
-        reduce_final(lax.rem(i + 2, 3))
-        return carry
-
-    lax.fori_loop(0, 3, finals, 0)
+    for p in range(parts):
+        for kind in (DOWN, GATE, UP):
+            reduce_final(3 * p + kind)
 
     def drain(i, carry):
         g, chip = i // nz, i % nz
@@ -391,9 +435,12 @@
 
         return carry
 
-    lax.fori_loop(0, 3 * nz, drain, 0)
+    lax.fori_loop(0, 3 * parts * nz, drain, 0)
     for step in range(1, n_tp):
         input_copy(lax.rem(tp + step, n_tp), tp).wait_send()
+
+
+PARTS = 1
 
 
 def fused_shards(tokens, cotangent, gate_weight, up_weight, down_weight):
@@ -401,51 +448,55 @@
     nz = n // 2
     count, width = tokens.shape
     rows, hidden = gate_weight.shape
+    height = hidden // PARTS
+    pieces = 3 * PARTS
     share = width // n_tp
     bf16, f32 = jnp.bfloat16, jnp.float32
     dma = pltpu.SemaphoreType.DMA
-    input_grad, grads = pl.pallas_call(
-        functools.partial(kernel, n, n_tp),
+    input_grad, gate_grad, up_grad, down_grad = pl.pallas_call(
+        functools.partial(kernel, n, n_tp, PARTS),
         out_shape=(
             jax.ShapeDtypeStruct((count, share), bf16),
-            jax.ShapeDtypeStruct((3, rows, hidden), f32),
-        ),
+        ) + (jax.ShapeDtypeStruct((hidden, rows), f32),) * 3,
         in_specs=[pl.BlockSpec(memory_space=pl.ANY)] * 5,
-        out_specs=(pl.BlockSpec(memory_space=pltpu.VMEM),) * 2,
+        out_specs=(pl.BlockSpec(memory_space=pltpu.VMEM),) * 4,
         scratch_shapes=[
             pltpu.VMEM((2, count, width), bf16),
-            pltpu.VMEM((3, n, rows, hidden), bf16),
-            pltpu.VMEM((3, count, hidden), f32),
-            pltpu.VMEM((3, count, hidden), bf16),
-            pltpu.VMEM((3, nz, rows, hidden), bf16),
-            pltpu.VMEM((3, nz, rows, hidden), bf16),
-            pltpu.VMEM((3, nz, rows, hidden), bf16),
-            pltpu.VMEM((3, 2, nz, rows, hidden), bf16),
-            pltpu.VMEM((rows, hidden), f32),
+            pltpu.VMEM((pieces, n, height, rows), bf16),
+            pltpu.VMEM((3, height, count), f32),
+            pltpu.VMEM((pieces, height, count), bf16),
+            pltpu.VMEM((pieces, height, rows), f32),
+            pltpu.VMEM((pieces, nz, height, rows), bf16),
+            pltpu.VMEM((pieces, nz, height, rows), bf16),
+            pltpu.VMEM((pieces, nz, height, rows), bf16),
+            pltpu.VMEM((pieces, 2, nz, height, rows), bf16),
+            pltpu.VMEM((height, rows), f32),
             pltpu.VMEM((n_tp, count, share), bf16),
             pltpu.VMEM((n_tp, count, share), bf16),
-            dma((5,)),
-            dma((3, 3, nz)),
-            dma((3, n)),
-            dma((3, nz)),
-            dma((3, nz)),
-            dma((3, nz)),
-            dma((3, 2, nz)),
+            dma((pieces + 2,)),
+            dma((pieces, 3, nz)),
+            dma((pieces, n)),
+            dma((pieces, nz)),
+            dma((pieces, nz)),
+            dma((pieces, nz)),
+            dma((pieces, 2, nz)),
             dma((n_tp,)),
             dma((n_tp,)),
         ],
         compiler_params=pltpu.CompilerParams(
             collective_id=0, has_side_effects=True, vmem_limit_bytes=67043328
         ),
-    )(tokens, cotangent, gate_weight, up_weight, down_weight)
-    return input_grad, grads[0], grads[1], grads[2]
+    )(tokens, cotangent, gate_weight.T, up_weight.T, down_weight.T)
+    return input_grad, gate_grad.T, up_grad.T, down_grad.T
 
 
 def shards(tokens, cotangent, gate_weight, up_weight, down_weight):
     n, n_tp = lax.axis_size("fs"), lax.axis_size("tp")
     rows = gate_weight.shape[0]
     share = tokens.shape[1] // n_tp
-    if n % 2 == 0 and rows % 128 == 0 and share % rows == 0 and n <= 8:
+    if n % 2 == 0 and rows % 128 == 0 and share % rows == 0 and n <= 8 and (
+        gate_weight.shape[1] % (16 * PARTS) == 0
+    ):
         return fused_shards(tokens, cotangent, gate_weight, up_weight, down_weight)
     return plain_shards(tokens, cotangent, gate_weight, up_weight, down_weight)
 

time: 165 us -> 147 us (0.89)
  Pallas kernels: 151 us -> 140 us
  local copies, waits for them, and re-layouts: 11.6 us -> 5.71 us
    pallas_call x1, Pallas kernels: 151 us -> 140 us  [fused_shards(): pl.pallas_call(functools.partial(kernel, n, n_tp, PARTS), out_shape=(jax....]
    unnamed x9 -> x8, local copies, waits for them, and re-layouts: 9.84 us -> 5.71 us
    squeeze x1 -> x0, local copies, waits for them, and re-layouts: 1.76 us -> none  [fused_shards(): return (input_grad, grads[0], grads[1], grads[2])]
where the time goes in v2:
time: 147 us; the launch traced here: 146 us
  Pallas kernels  140 us (95%)
  local copies, waits for them, and re-layouts  5.71 us (4%)
    pallas_call x1, Pallas kernels, fused_shards(): pl.pallas_call(functools.partial(kernel, n, n_tp, PARTS), out_shape=(jax....  140 us
    unnamed x8, local copies, waits for them, and re-layouts  5.71 us

profile of v2, /device:TPU:10, one launch (start us, length us, event | category | flops | bytes accessed | tf_op | source)
XLA Modules:
  0.0 146.4 jit_solution(13418867880612851183)
XLA Ops:
  0.6 140.0 %shard_map.84 = (bf16[512,512]{1,0:T(8,128)(2,1)}, f32[704,256]{1,0:T(8,128)}, f32[704,256]{1,0:T(8,128)}, f32[704,256]{1,0:T(8,128)}) custom-call(bf16[512,2048]{1,0:T(8,128)(2,1)} %tok.1, bf16[512,2048]{1,0:T(8,128)(2,1)} %cot.1, bf16[704,256]{1,0:T(8,128)(2,1)} %bitcast.9, bf16[704,256]{1,0:T(8,128)(2,1)} %bitcast.10, bf16[704,256]{1,0:T(8,128)(2,1)} %bitcast.11), custom_call_target="tpu_custom_call" | custom-call | tf_op jit(solution)/shard_map/pallas_call | solution.py:456
  140.6 0.0 copy-start.1
  140.6 0.0 copy-start
  140.6 2.0 %copy.13 = bf16[512,512]{1,0:T(8,128)(2,1)} copy(bf16[512,512]{1,0:T(8,128)(2,1)} %get-tuple-element.16) | data formatting | bytes 1048576
  142.6 2.0 %copy.14 = f32[256,704]{0,1:T(8,128)} copy(f32[256,704]{0,1:T(8,128)} %bitcast.8) | data formatting | bytes 1441792
  144.6 0.0 copy-done.1
  144.6 0.9 copy.15
  145.5 0.0 copy-done
  145.5 0.9 copy.16
Async XLA Ops:
  140.6 4.0 %copy-start.1 = (f32[704,256]{1,0:T(8,128)S(1)}, f32[704,256]{1,0:T(8,128)}, u32[]{:S(2)}) copy-start(f32[704,256]{1,0:T(8,128)} %get-tuple-element.10) | copy-start | bytes 2162692
  140.6 4.9 %copy-start = (f32[704,256]{1,0:T(8,128)S(1)}, f32[704,256]{1,0:T(8,128)}, u32[]{:S(2)}) copy-start(f32[704,256]{1,0:T(8,128)} %get-tuple-element.11) | copy-start | bytes 2162692

commit v3 on v2

--- a/solution.py
+++ b/solution.py
@@ -68,6 +68,7 @@
 
 
 MESH = pl.DeviceIdType.MESH
+LAG = 2
 GATE, UP, DOWN = 0, 1, 2
 RIGHT, LEFT, SIBLING = 0, 1, 2
 
@@ -356,13 +357,17 @@
 
         by_rows(strip)
 
+    def in_turn(i):
+        return 3 * (i // 3) + (i + 2) % 3
+
     def gather_and_reduce(t, carry):
         kind = t % 3
         g = jnp.where(kind == DOWN, t, t - 3)
         acc[kind] = jnp.zeros(acc.shape[1:], acc.dtype)
         reduce_all(g, jnp.logical_and(g >= 0, is_end))
         gather(t)
-        reduce_all(g, jnp.logical_and(g >= 0, jnp.logical_not(is_end)))
+        turn = t - 2 - LAG
+        reduce_all(in_turn(turn), jnp.logical_and(turn >= 0, jnp.logical_not(is_end)))
 
         @pl.when(kind == UP)
         def _():
@@ -376,6 +381,12 @@
 
     lax.fori_loop(0, 3 * parts, gather_and_reduce, 0)
     last = 3 * parts - 3
+
+    def catch_up(turn, carry):
+        reduce_all(in_turn(turn), jnp.logical_not(is_end))
+        return carry
+
+    lax.fori_loop(max(3 * parts - 2 - LAG, 0), 3 * parts - 2, catch_up, 0)
     steps = max(nz - 1, 1)
 
     def last_two(i, carry):
@@ -385,11 +396,15 @@
         def _():
             sibling_terms(g)
 
+        @pl.when(jnp.logical_and(i < n_tp, jnp.logical_not(is_end)))
+        def _():
+            input_part(i)
+
         @pl.when(i < 2 * (nz - 1))
         def _():
             reduce_step(g, i % steps + 1)
 
-        @pl.when(i < n_tp)
+        @pl.when(jnp.logical_and(i < n_tp, is_end))
         def _():
             input_part(i)
 
@@ -440,7 +455,7 @@
         input_copy(lax.rem(tp + step, n_tp), tp).wait_send()
 
 
-PARTS = 1
+PARTS = 2
 
 
 def fused_shards(tokens, cotangent, gate_weight, up_weight, down_weight):

time: 147 us -> 144 us (0.980)
  Pallas kernels: 140 us -> 138 us
    pallas_call x1, Pallas kernels: 140 us -> 138 us  [fused_shards(): pl.pallas_call(functools.partial(kernel, n, n_tp, PARTS), out_shape=(jax....]
where the time goes in v3:
time: 144 us
  Pallas kernels  138 us (96%)
  local copies, waits for them, and re-layouts  5.71 us (4%)
    pallas_call x1, Pallas kernels, fused_shards(): pl.pallas_call(functools.partial(kernel, n, n_tp, PARTS), out_shape=(jax....  138 us
    unnamed x8, local copies, waits for them, and re-layouts  5.71 us

profile of v3, /device:TPU:10, one launch (start us, length us, event | category | flops | bytes accessed | tf_op | source)
XLA Modules:
  0.0 144.3 jit_solution(360621216593345686)
XLA Ops:
  0.6 137.9 %shard_map.84 = (bf16[512,512]{1,0:T(8,128)(2,1)}, f32[704,256]{1,0:T(8,128)}, f32[704,256]{1,0:T(8,128)}, f32[704,256]{1,0:T(8,128)}) custom-call(bf16[512,2048]{1,0:T(8,128)(2,1)} %tok.1, bf16[512,2048]{1,0:T(8,128)(2,1)} %cot.1, bf16[704,256]{1,0:T(8,128)(2,1)} %bitcast.9, bf16[704,256]{1,0:T(8,128)(2,1)} %bitcast.10, bf16[704,256]{1,0:T(8,128)(2,1)} %bitcast.11), custom_call_target="tpu_custom_call" | custom-call | tf_op jit(solution)/shard_map/pallas_call | solution.py:471
  138.5 0.0 copy-start.1
  138.5 0.0 copy-start
  138.6 2.0 %copy.13 = bf16[512,512]{1,0:T(8,128)(2,1)} copy(bf16[512,512]{1,0:T(8,128)(2,1)} %get-tuple-element.16) | data formatting | bytes 1048576
  140.5 2.0 %copy.14 = f32[256,704]{0,1:T(8,128)} copy(f32[256,704]{0,1:T(8,128)} %bitcast.8) | data formatting | bytes 1441792
  142.5 0.0 copy-done.1
  142.5 0.9 copy.15
  143.4 0.0 copy-done
  143.4 0.9 copy.16
Async XLA Ops:
  138.5 4.0 %copy-start.1 = (f32[704,256]{1,0:T(8,128)S(1)}, f32[704,256]{1,0:T(8,128)}, u32[]{:S(2)}) copy-start(f32[704,256]{1,0:T(8,128)} %get-tuple-element.10) | copy-start | bytes 2162692
  138.5 4.9 %copy-start = (f32[704,256]{1,0:T(8,128)S(1)}, f32[704,256]{1,0:T(8,128)}, u32[]{:S(2)}) copy-start(f32[704,256]{1,0:T(8,128)} %get-tuple-element.11) | copy-start | bytes 2162692
